TPU v7x, 32 devices: a whole 2x2x4 slice. The times are simulated.
32 devices in a mesh: sp: 4 (over y, x), tp: 8 (over z, core).
Axes of the slice: x: 2, y: 2, z: 4, core: 2. Of those that a mesh axis runs over, the one named last changes fastest.
Arguments:
- lru_input: bfloat16 [1024, 2048], P('sp', 'tp'), may hold values from -27 to 27
- gate_input: bfloat16 [1024, 2048], P('sp', 'tp'), may hold values from -6 to 6
- documents: int32 [1024], P('sp'), may hold values from 0 to 1, never falling along the last dimension, each value on 1 to 768 neighbouring positions
- conv_taps: bfloat16 [4, 2048], P(None, 'tp'), may hold values from -3 to 3
- rate_weight: bfloat16 [16, 128, 128], P('tp'), may hold values from -0.5 to 0.5
- inlet_weight: bfloat16 [16, 128, 128], P('tp'), may hold values from -0.5 to 0.5
- decay_param: float32 [2048], P('tp')
- lru_gain: float32 [2048], P('tp'), may hold values from 0.1 to 1.9
- out_weight: bfloat16 [2048, 2048], P('tp'), may hold values from -0.125 to 0.125
- residual: bfloat16 [1024, 2048], P('sp'), may hold values from -6 to 6
- ffn_gain: float32 [2048], replicated, may hold values from 0.1 to 1.9
- routes: int32 [1024, 2], P('sp'), may hold values from 0 to 3, all different within a row; in each aligned block of 32 rows (0 to 31, 32 to 63, ...) at most 32 rows name the same one
- route_weights: float32 [1024, 2], P('sp'), may hold values from 0.1 to 0.9
- w_gate: bfloat16 [4, 2048, 6144], P('sp', None, 'tp'), may hold values from -0.125 to 0.125
- w_up: bfloat16 [4, 2048, 6144], P('sp', None, 'tp'), may hold values from -0.125 to 0.125
- w_down: bfloat16 [4, 6144, 2048], P('sp', 'tp'), may hold values from -0.078125 to 0.078125
Outputs:
- mixed_out: bfloat16 [1024, 2048], P(('sp', 'tp'))
Inputs may be any that keep to these rules, and one draw needn't show every extreme that they name: `documents`: document numbers start at 0 and never fall along the sequence; a document spans at most 768 positions. `routes`: each row names 2 different experts. In each aligned block of 32 rows no expert is named by more than 32 rows, a bound that some block reaches.
All inputs are finite; a program needn't handle non-finite values.
Results may differ from a plain program's by a relative error of at most 0.017.
Values may be sent and summed in bfloat16 or wider, within the bound.
A program may use at most 64 MiB of HBM per device.

v0:
```python
import jax
import jax.numpy as jnp
from jax import lax
from jax.sharding import PartitionSpec as P

D_RNN = 2048


EPSILON = 1e-06
RATE_SCALE = 8.0


def shifted(block, axis, distance):
    devices = range(lax.axis_size(axis))
    route = [(i - distance, i) for i in devices if i - distance in devices]
    return lax.ppermute(block, axis, route)


def carried_in(value, axis, join, neutral):
    count, mine = (lax.axis_size(axis), lax.axis_index(axis))
    pieces = jax.tree.map(lambda part: lax.all_gather(part, axis), value)
    so_far = jax.tree.map(
        lambda part, zero: jnp.full_like(part, 0) + jnp.asarray(zero, part.dtype), value, neutral
    )

    def hop(position, so_far):
        longer = join(so_far, jax.tree.map(lambda part: part[position], pieces))
        return jax.tree.map(lambda new, old: jnp.where(position < mine, new, old), longer, so_far)

    return lax.fori_loop(0, count - 1, hop, so_far)


def join_runs(earlier_run, later_run):
    return (earlier_run[0] * later_run[0], later_run[0] * earlier_run[1] + later_run[1])


def slot_targets(route_block, expert_count, capacity):
    flat_routes = route_block.reshape(-1)
    onehot = (flat_routes[:, None] == jnp.arange(expert_count, dtype=jnp.int32)[None, :]).astype(
        jnp.int32
    )
    earlier_hits = jnp.cumsum(onehot, axis=0) - onehot
    slot_index = jnp.sum(earlier_hits * onehot, axis=1)
    return (flat_routes * capacity + slot_index).reshape(route_block.shape)


def pick_matrix(targets, slot_total):
    slot_hits = targets[None, :, :] == jnp.arange(slot_total, dtype=jnp.int32)[:, None, None]
    return jnp.sum(slot_hits.astype(jnp.int32), axis=2).astype(jnp.bfloat16)


def rms_rows(row_block, gain_vector):
    floated = row_block.astype(jnp.float32)
    inverse_rms = lax.rsqrt(jnp.mean(floated * floated, axis=1, keepdims=True) + EPSILON)
    return (floated * inverse_rms * gain_vector[None, :]).astype(jnp.bfloat16)


def expert_apply(row_piece, gate_weight, up_weight, down_weight):
    gate_part = jnp.dot(row_piece, gate_weight, preferred_element_type=jnp.float32)
    up_part = jnp.dot(row_piece, up_weight, preferred_element_type=jnp.float32)
    hidden_units = (jax.nn.silu(gate_part) * up_part).astype(jnp.bfloat16)
    return jnp.dot(hidden_units, down_weight, preferred_element_type=jnp.float32)


def local(
    lru_input,
    gate_input,
    documents,
    conv_taps,
    rate_weight,
    inlet_weight,
    decay_param,
    lru_gain,
    out_weight,
    residual,
    ffn_gain,
    routes,
    route_weights,
    w_gate,
    w_up,
    w_down,
):
    positions = lru_input.shape[0]
    channels = lru_input.shape[1]
    model_width = residual.shape[1]
    reach_back = conv_taps.shape[0] - 1
    tail_rows, tail_docs = shifted(
        (lru_input[positions - reach_back :], documents[positions - reach_back :] + 1), "sp", 1
    )
    prior_docs = jnp.concatenate([tail_docs - 1, documents])
    padded_input = jnp.concatenate([tail_rows, lru_input], axis=0)
    conv_sum = jnp.zeros((positions, channels), jnp.float32)
    for tap_index in range(reach_back + 1):
        same_doc = (prior_docs[tap_index : tap_index + positions] == documents).astype(jnp.float32)[
            :, None
        ]
        conv_sum = (
            conv_sum
            + padded_input[tap_index : tap_index + positions].astype(jnp.float32)
            * conv_taps[tap_index].astype(jnp.float32)[None, :]
            * same_doc
        )
    convolved = conv_sum.astype(jnp.bfloat16)
    grouped = convolved.reshape(positions, rate_weight.shape[0], rate_weight.shape[1])
    rate_gate = jax.nn.sigmoid(
        jnp.einsum(
            "tnc,ncd->tnd", grouped, rate_weight, preferred_element_type=jnp.float32
        ).reshape(positions, channels)
    )
    inlet_gate = jax.nn.sigmoid(
        jnp.einsum(
            "tnc,ncd->tnd", grouped, inlet_weight, preferred_element_type=jnp.float32
        ).reshape(positions, channels)
    )
    log_decay = -RATE_SCALE * rate_gate * jax.nn.softplus(-decay_param)[None, :]
    starts = (prior_docs[reach_back - 1 : reach_back - 1 + positions] != documents)[:, None]
    decay_step = jnp.where(starts, 0.0, jnp.exp(log_decay))
    norm_factor = jnp.where(starts, 1.0, jnp.sqrt(-jnp.expm1(2.0 * log_decay)))
    drive_term = norm_factor * inlet_gate * convolved.astype(jnp.float32)
    decay_run, local_state = lax.associative_scan(join_runs, (decay_step, drive_term), axis=0)
    carried = carried_in(
        (decay_run[positions - 1], local_state[positions - 1]),
        "sp",
        join_runs,
        (jnp.ones((channels,), jnp.float32), jnp.zeros((channels,), jnp.float32)),
    )
    hidden_state = local_state + decay_run * carried[1][None, :]
    square_sums = lax.psum(jnp.sum(hidden_state * hidden_state, axis=1), "tp")
    inverse_rms = lax.rsqrt(square_sums[:, None] / D_RNN + EPSILON)
    mixer_rows = (
        hidden_state * inverse_rms * lru_gain[None, :] * jax.nn.gelu(gate_input.astype(jnp.float32))
    ).astype(jnp.bfloat16)
    tp_count = lax.axis_size("tp")
    tp_here = lax.axis_index("tp")
    expert_count = lax.axis_size("sp")
    route_rows = positions // tp_count
    top_count = routes.shape[1]
    capacity = 2 * top_count * route_rows // expert_count
    slot_total = expert_count * capacity
    projected = lax.psum_scatter(
        jnp.dot(mixer_rows, out_weight, preferred_element_type=jnp.float32).astype(jnp.bfloat16),
        "tp",
        scatter_dimension=0,
        tiled=True,
    ).astype(jnp.float32)
    own_rows = (
        lax.dynamic_slice_in_dim(residual, tp_here * route_rows, route_rows, 0).astype(jnp.float32)
        + projected
    ).astype(jnp.bfloat16)
    own_routes = lax.dynamic_slice_in_dim(routes, tp_here * route_rows, route_rows, 0)
    targets = slot_targets(own_routes, expert_count, capacity)
    outgoing = jnp.dot(
        pick_matrix(targets, slot_total),
        rms_rows(own_rows, ffn_gain),
        preferred_element_type=jnp.float32,
    ).astype(jnp.bfloat16)
    arrived = lax.all_to_all(
        outgoing.reshape(expert_count, capacity, model_width),
        "sp",
        split_axis=0,
        concat_axis=0,
        tiled=True,
    )
    partial_out = expert_apply(
        lax.all_gather(arrived.reshape(slot_total, model_width), "tp", axis=0, tiled=True),
        w_gate[0],
        w_up[0],
        w_down[0],
    )
    expert_out = lax.psum_scatter(
        partial_out.astype(jnp.bfloat16), "tp", scatter_dimension=0, tiled=True
    )
    returned = lax.all_to_all(
        expert_out.reshape(expert_count, capacity, model_width),
        "sp",
        split_axis=0,
        concat_axis=0,
        tiled=True,
    )
    picked = returned.reshape(slot_total, model_width)[targets.reshape(-1)].astype(jnp.float32)
    picked = picked.reshape(route_rows, top_count, model_width)
    own_weights = lax.dynamic_slice_in_dim(route_weights, tp_here * route_rows, route_rows, 0)
    routed = jnp.sum(picked * own_weights[:, :, None], axis=1)
    return (own_rows.astype(jnp.float32) + routed).astype(jnp.bfloat16)


def solution(mesh):
    return jax.shard_map(
        local,
        mesh=mesh,
        in_specs=(
            P("sp", "tp"),
            P("sp", "tp"),
            P("sp"),
            P(None, "tp"),
            P("tp", None, None),
            P("tp", None, None),
            P("tp"),
            P("tp"),
            P("tp", None),
            P("sp", None),
            P(),
            P("sp", None),
            P("sp", None),
            P("sp", None, "tp"),
            P("sp", None, "tp"),
            P("sp", "tp", None),
        ),
        out_specs=P(("sp", "tp"), None),
        check_vma=False,
    )
```

profile of v0, /device:TPU:0, one launch (start us, length us, event | category | flops | bytes accessed | tf_op | source)
XLA Modules:
  0.0 344.2 jit_solution(4255377633194049739)
XLA Ops:
  7.4 5.0 %collective-permute-start = (s32[3]{0:T(128)S(1)}, s32[3]{0:T(128)S(1)}, u32[]{:S(2)}, u32[]{:S(2)}) collective-permute-start(s32[3]{0:T(128)S(1)} %slice_add_fusion.2), channel_id=1, source_target_pairs={{0,8},{8,16},{16,24},{1,9},{9,17},{17,25},{2,10},{10,18},{18,26},{... | collective-permute-start | bytes 44 | tf_op jit(solution)/shard_map/ppermute | solution.py:16
  13.1 3.4 collective-permute-start.1
  19.6 1.3 add_convert_fusion.1
  24.8 1.9 convert_multiply_fusion.5
  26.8 1.6 slice.288
  28.4 1.6 slice.289
  31.4 1.8 multiply_add_fusion.1
  33.2 1.5 slice.294
  34.7 1.5 slice.295
  37.5 1.6 multiply_add_fusion.2
  39.1 1.5 slice.300
  40.5 1.4 slice.301
  42.0 1.4 slice.299
  43.4 1.4 slice.303
  44.9 1.4 multiply_add_fusion.3
  46.3 1.4 slice.306
  47.7 1.4 slice.307
  49.0 1.4 slice.305
  50.4 1.4 slice.309
  51.8 1.4 multiply_add_fusion.4
  54.3 1.3 slice.311
  55.6 1.3 slice.315
  56.9 1.3 multiply_add_fusion.5
  58.3 1.3 slice.318
  59.6 1.3 slice.319
  60.9 1.3 slice.317
  62.2 1.3 slice.321
  63.5 1.3 multiply_add_fusion.6
  70.7 1.4 fusion.62
  72.6 1.3 slice.316
  73.9 1.3 slice.333
  75.2 1.3 slice.398
  76.5 1.3 slice.372
  77.8 1.3 slice.310
  79.7 1.3 slice.397
  82.3 1.4 slice.337
  86.2 1.5 slice.298
  87.6 1.5 slice.339
  92.3 1.5 slice.341
  93.8 1.3 slice.368
  96.5 1.6 slice.343
  111.3 1.5 fusion.43
  113.8 1.5 pad_maximum_fusion.4
  115.3 2.2 pad.126
  118.1 1.6 add.331
  119.7 1.7 fusion.32
  121.5 2.3 pad.113
  124.5 8.1 %all-gather.1 = f32[4,1,256]{2,1,0:T(1,128)S(1)} all-gather(f32[1,1,256]{2,1,0:T(1,128)S(1)} %add_bitcast_fusion), channel_id=1, replica_groups=mesh['sp'=4,'tp'=8] {'sp'}, dimensions={0}, use_global_device_ids=true | all-gather | bytes 5120 | tf_op jit(solution)/shard_map/all_gather | solution.py:21
  133.5 1.5 pad.128
  134.9 2.3 pad.129
  138.0 7.1 %all-gather = f32[4,1,256]{2,1,0:T(1,128)S(1)} all-gather(f32[1,1,256]{2,1,0:T(1,128)S(1)} %add_bitcast_fusion.1), channel_id=1, replica_groups=mesh['sp'=4,'tp'=8] {'sp'}, dimensions={0}, use_global_device_ids=true | all-gather | bytes 5120 | tf_op jit(solution)/shard_map/all_gather | solution.py:21
  145.2 1.9 multiply_reduce_fusion.1
  147.1 13.6 %psum.7 = f32[256]{0:T(256)S(1)} all-reduce(f32[256]{0:T(256)S(1)} %get-tuple-element.130), channel_id=1, replica_groups=mesh['sp'=4,'tp'=8] {'tp'}, use_global_device_ids=true, to_apply=%region_3.4 | all-reduce | flops 256 | bytes 2048 | tf_op jit(solution)/shard_map/psum | solution.py:128
  160.7 2.9 convolution_convert_fusion.1
  165.3 28.4 %reduce-scatter.3.cloned.1.call-done = bf16[32,2048]{1,0:T(8,128)(2,1)} async-done(((bf16[256,2048]{1,0:T(8,128)(2,1)}), bf16[32,2048]{1,0:T(8,128)(2,1)}) %reduce-scatter.3.cloned.1.call-update) | async-done | bytes 131088 | tf_op jit(solution)/shard_map/reduce_scatter | solution.py:140
  195.2 10.7 %all_to_all.10 = bf16[4,32,2048]{2,1,0:T(8,128)(2,1)} all-to-all(bf16[4,32,2048]{2,1,0:T(8,128)(2,1)S(1)} %bitcast.67), channel_id=1, replica_groups=mesh['sp'=4,'tp'=8] {'sp'}, dimensions={0} | all-to-all | bytes 1048576 | tf_op jit(solution)/shard_map/all_to_all | solution.py:157
  206.0 45.6 %all-gather.4.cloned.1.call-done = bf16[1024,2048]{1,0:T(8,128)(2,1)} async-done(((bf16[128,2048]{1,0:T(8,128)(2,1)}), bf16[1024,2048]{1,0:T(8,128)(2,1)}) %all-gather.4.cloned.1.call-update) | async-done | bytes 4194320 | tf_op jit(solution)/shard_map/all_gather | solution.py:165
  251.5 8.3 %fusion.1 = f32[1024,768]{1,0:T(8,128)} fusion(bf16[1024,2048]{1,0:T(8,128)(2,1)} %all-gather.4.cloned.1.call-done, bf16[1,2048,768]{2,1,0:T(8,128)(2,1)} %param.32), kind=kOutput, calls=%fused_computation.6 | convolution fusion | flops 3221225472 | bytes 10485760 | tf_op jit(solution)/shard_map/dot_general | solution.py:60
  259.8 12.3 %convolution_convert_fusion = bf16[1024,2048]{1,0:T(8,128)(2,1)} fusion(bf16[1,768,2048]{2,1,0:T(8,128)(2,1)S(1)} %copy-done, f32[1024,768]{1,0:T(8,128)} %fusion.1, bf16[1024,2048]{1,0:T(8,128)(2,1)} %all-gather.4.cloned.1.call-done, bf16[1,2048,768]{2,1,0:T(8,128)(2,1)} %param.31), kind=kOutput, calls=%fused_computation.4 | convolution fusion | flops 6449266688 | bytes 17825792 | tf_op jit(solution)/shard_map/dot_general | solution.py:62
  272.3 48.8 %reduce-scatter.5.cloned.1.call-done = bf16[128,2048]{1,0:T(8,128)(2,1)} async-done(((bf16[1024,2048]{1,0:T(8,128)(2,1)}), bf16[128,2048]{1,0:T(8,128)(2,1)}) %reduce-scatter.5.cloned.1.call-update) | async-done | bytes 524304 | tf_op jit(solution)/shard_map/reduce_scatter | solution.py:170
  321.1 4.1 %all-to-all-start.1 = ((bf16[4,32,2048]{2,1,0:T(8,128)(2,1)}), bf16[4,32,2048]{2,1,0:T(8,128)(2,1)}, u32[]{:S(2)}, u32[]{:S(2)}) async-start(bf16[4,32,2048]{2,1,0:T(8,128)(2,1)} %bitcast.68), calls=%async_computation.3 | async-start | bytes 1048576 | tf_op jit(solution)/shard_map/all_to_all | solution.py:173
  326.0 5.9 %all-to-all-done.1 = bf16[4,32,2048]{2,1,0:T(8,128)(2,1)} async-done(((bf16[4,32,2048]{2,1,0:T(8,128)(2,1)}), bf16[4,32,2048]{2,1,0:T(8,128)(2,1)}, u32[]{:S(2)}, u32[]{:S(2)}) %all-to-all-start.1) | async-done | bytes 524320 | tf_op jit(solution)/shard_map/all_to_all | solution.py:173
  331.9 2.2 gather_fusion
  335.2 1.8 multiply_reduce_fusion
  (144 shorter events, 50.9 us)
Async XLA Ops:
  6.5 253.3 %copy-start = (bf16[1,768,2048]{2,1,0:T(8,128)(2,1)S(1)}, bf16[1,768,2048]{2,1,0:T(8,128)(2,1)}, u32[]{:S(2)}) copy-start(bf16[1,768,2048]{2,1,0:T(8,128)(2,1)} %param.33) | copy-start | bytes 9437188
  6.5 187.1 %reduce-scatter.3.cloned.1.call-start = ((), (), s32[]{:S(2)}) async-start(), calls=%async_computation.4 | async-start | bytes 1179648 | tf_op jit(solution)/shard_map/reduce_scatter | solution.py:140
  7.4 10.6 %collective-permute-start = (s32[3]{0:T(128)S(1)}, s32[3]{0:T(128)S(1)}, u32[]{:S(2)}, u32[]{:S(2)}) collective-permute-start(s32[3]{0:T(128)S(1)} %slice_add_fusion.2), channel_id=1, source_target_pairs={{0,8},{8,16},{16,24},{1,9},{9,17},{17,25},{2,10},{10,18},{18,26},{... | collective-permute-start | bytes 44 | tf_op jit(solution)/shard_map/ppermute | solution.py:16
  13.1 6.5 %collective-permute-start.1 = (bf16[3,256]{1,0:T(4,128)(2,1)S(1)}, bf16[3,256]{1,0:T(4,128)(2,1)S(1)}, u32[]{:S(2)}, u32[]{:S(2)}) collective-permute-start(bf16[3,256]{1,0:T(4,128)(2,1)S(1)} %slice.275), channel_id=1, source_target_pairs={{0,8},{8,16},{16,24},{1,9},{9,17},{17,25},{2,10},{10,18},{18,26},{... | collective-permute-start | bytes 4616 | tf_op jit(solution)/shard_map/ppermute | solution.py:16
  95.7 17.1 %copy-start.5 = (f32[1,256]{1,0:T(1,128)S(1)}, f32[1,256]{1,0:T(1,128)}, u32[]{:S(2)}) copy-start(f32[1,256]{1,0:T(1,128)} %slice.368) | copy-start | bytes 3076
  107.0 14.3 %copy-start.4 = (f32[1,256]{1,0:T(1,128)S(1)}, f32[1,256]{1,0:T(1,128)}, u32[]{:S(2)}) copy-start(f32[1,256]{1,0:T(1,128)} %slice.367) | copy-start | bytes 3076
  107.0 25.5 %copy-start.3 = (f32[1,256]{1,0:T(1,128)S(1)}, f32[1,256]{1,0:T(1,128)}, u32[]{:S(2)}) copy-start(f32[1,256]{1,0:T(1,128)} %slice.393) | copy-start | bytes 3076
  109.9 35.2 %copy-start.1 = (f32[256]{0:T(256)S(1)}, f32[256]{0:T(256)}, u32[]{:S(2)}) copy-start(f32[256]{0:T(256)} %custom-call) | copy-start | bytes 3076
  112.9 47.8 %copy-start.6 = (f32[256]{0:T(256)S(1)}, f32[256]{0:T(256)}, u32[]{:S(2)}) copy-start(f32[256]{0:T(256)} %param.25) | copy-start | bytes 3076
  134.9 59.9 %copy-start.2 = (f32[2048]{0:T(1024)S(1)}, f32[2048]{0:T(1024)}, u32[]{:S(2)}) copy-start(f32[2048]{0:T(1024)} %param.28) | copy-start | bytes 24580
  163.6 87.9 %all-gather.4.cloned.1.call-start = ((), (), s32[]{:S(2)}) async-start(), calls=%async_computation.5 | async-start | bytes 4718592 | tf_op jit(solution)/shard_map/all_gather | solution.py:165
  205.9 115.2 %reduce-scatter.5.cloned.1.call-start = ((), (), s32[]{:S(2)}) async-start(), calls=%async_computation.6 | async-start | bytes 4718592 | tf_op jit(solution)/shard_map/reduce_scatter | solution.py:170
  272.2 53.1 %copy-start.7 = (f32[256,2]{0,1:T(2,128)S(1)}, f32[256,2]{0,1:T(2,128)}, u32[]{:S(2)}) copy-start(f32[256,2]{0,1:T(2,128)} %param.30) | copy-start | bytes 6148
  321.1 10.8 %all-to-all-start.1 = ((bf16[4,32,2048]{2,1,0:T(8,128)(2,1)}), bf16[4,32,2048]{2,1,0:T(8,128)(2,1)}, u32[]{:S(2)}, u32[]{:S(2)}) async-start(bf16[4,32,2048]{2,1,0:T(8,128)(2,1)} %bitcast.68), calls=%async_computation.3 | async-start | bytes 1048576 | tf_op jit(solution)/shard_map/all_to_all | solution.py:173
Sparse Core Ops, SparseCore 0:
  163.7 29.8 reduce-scatter.2
  206.1 45.4 all-gather.3
  272.3 48.7 reduce-scatter.4
where the time goes:
time: 348 us; the launch traced here: 344 us
  waiting for transfers between devices  129 us (37%)
  local copies, waits for them, and re-layouts  79.5 us (23%)
  other arithmetic  44.3 us (13%)
  blocking collectives  39.5 us (11%)
  matrix products  26.1 us (8%)
  between operations  13.5 us (4%)
  starting transfers between devices  12.6 us (4%)
    slice x52, local copies, waits for them, and re-layouts, local(): lax.associative_scan(join_runs, (decay_step, drive_term), axis=0)  61.6 us
    reduce_scatter x1, waiting for transfers between devices, local(): lax.psum_scatter(partial_out.astype(jnp.bfloat16), 'tp', scatter_dimensio...  48.8 us
    all_gather x1, waiting for transfers between devices, local(): lax.all_gather(arrived.reshape(slot_total, model_width), 'tp', axis=0, ti...  45.6 us
    reduce_scatter x1, waiting for transfers between devices, local(): lax.psum_scatter(jnp.dot(mixer_rows, out_weight, preferred_element_type=j...  28.4 us
    add x14, other arithmetic, join_runs(): later_run[0] * earlier_run[1] + later_run[1]  15.7 us
    all_gather x2, blocking collectives, carried_in(): pieces = jax.tree.map(lambda part: lax.all_gather(part, axis), value)  15.1 us
    psum x1, blocking collectives, local(): square_sums = lax.psum(jnp.sum(hidden_state * hidden_state, axis=1), 'tp')  13.6 us
    dot_general x1, matrix products, expert_apply(): jnp.dot(hidden_units, down_weight, preferred_element_type=jnp.float32)  12.3 us
  transfers between devices with their start and end apart: 6, of which 4 were waited for; matrix products, arithmetic and copies ran while one was open for 2% of the time, Pallas kernels for 0%

commit v1 on v0

--- a/solution.py
+++ b/solution.py
@@ -1,6 +1,10 @@
+import functools
+
 import jax
 import jax.numpy as jnp
 from jax import lax
+from jax.experimental import pallas as pl
+from jax.experimental.pallas import tpu as pltpu
 from jax.sharding import PartitionSpec as P
 
 D_RNN = 2048
@@ -184,9 +188,620 @@
     return (own_rows.astype(jnp.float32) + routed).astype(jnp.bfloat16)
 
 
+MESH = pl.DeviceIdType.MESH
+LANES = 128
+GELU_SCALE = 0.7978845608028654
+
+
+def sender(source, target, send_sem, recv_sem, peer):
+    return pltpu.make_async_remote_copy(
+        src_ref=source,
+        dst_ref=target,
+        send_sem=send_sem,
+        recv_sem=recv_sem,
+        device_id=peer,
+        device_id_type=MESH,
+    )
+
+
+def greet(peers):
+    barrier = pltpu.get_barrier_semaphore()
+    for peer in peers:
+        pl.semaphore_signal(barrier, inc=1, device_id=peer, device_id_type=MESH)
+    pl.semaphore_wait(barrier, len(peers))
+
+
+def one_minus_exp(value):
+    series = 1.0 + value * (1.0 / 6.0)
+    for order in (5.0, 4.0, 3.0, 2.0):
+        series = 1.0 + value * (1.0 / order) * series
+    return jnp.where(value > -0.25, -value * series, 1.0 - jnp.exp(value))
+
+
+def down_by(block, distance, filler):
+    count = block.shape[0]
+    if distance % 8 == 0:
+        top = jnp.full((distance, block.shape[1]), filler, block.dtype)
+        return jnp.concatenate([top, block[: count - distance]], axis=0)
+    row = lax.broadcasted_iota(jnp.int32, block.shape, 0)
+    return jnp.where(row >= distance, pltpu.roll(block, distance, 0), filler)
+
+
+def front_kernel(
+    n_sp,
+    n_tp,
+    lru_ref,
+    gate_ref,
+    docs_ref,
+    taps_ref,
+    rate_ref,
+    inlet_ref,
+    decay_ref,
+    gain_ref,
+    out_w_ref,
+    residual_ref,
+    ffn_ref,
+    weights_ref,
+    own_ref,
+    normed_ref,
+    shares_ref,
+    halo_x,
+    halo_d,
+    carry_out,
+    carry_in,
+    share_in,
+    run_a,
+    run_b,
+    parts,
+    pair_in,
+    z_out,
+    z_in,
+    squares,
+    square_pair,
+    square_out,
+    square_in,
+    res_rows,
+    res_sem,
+    halo_s,
+    halo_r,
+    carry_s,
+    carry_r,
+    share_s,
+    share_r,
+    pair_s,
+    pair_r,
+    z_s,
+    z_r,
+):
+    me_s, me_t = lax.axis_index("sp"), lax.axis_index("tp")
+    n_z = n_tp // 2
+    me_z, me_c = me_t // 2, me_t % 2
+    rows, channels = lru_ref.shape
+    width = out_w_ref.shape[1]
+    piece = rows // n_tp
+    residual_copy = pltpu.make_async_copy(
+        residual_ref.at[pl.ds(pl.multiple_of(me_t * piece, piece), piece)], res_rows, res_sem
+    )
+    residual_copy.start()
+    sp_peers = [((me_s + k) % n_sp, me_t) for k in range(1, n_sp)]
+    tp_peers = [(me_s, (me_t + k) % n_tp) for k in range(1, n_tp)]
+    greet(sp_peers + tp_peers)
+    halo = [
+        sender(lru_ref.at[pl.ds(rows - 16, 16)], halo_x, halo_s.at[0], halo_r.at[0], sp_peers[0]),
+        sender(docs_ref.at[pl.ds(rows - 8, 8)], halo_d, halo_s.at[1], halo_r.at[1], sp_peers[0]),
+    ]
+    for copy in halo:
+        copy.start()
+    share = [
+        sender(weights_ref, share_in.at[me_s], share_s.at[k], share_r.at[k], peer)
+        for k, peer in enumerate(sp_peers)
+    ]
+    for copy in share:
+        copy.start()
+    for copy in halo:
+        copy.wait()
+
+    docs = docs_ref[...]
+    before = jnp.where(me_s == 0, jnp.int32(-1), halo_d[...])
+    docs_long = jnp.concatenate([before, docs], axis=0)
+    taps = taps_ref[...].astype(jnp.float32)
+    starts = docs_long[7 : 7 + rows] != docs
+    for group in range(channels // LANES):
+        span = slice(group * LANES, (group + 1) * LANES)
+        long = jnp.concatenate(
+            [halo_x[:, span].astype(jnp.float32)[8:], lru_ref[:, span].astype(jnp.float32)], axis=0
+        )
+        total = jnp.zeros((rows, LANES), jnp.float32)
+        for tap in range(taps.shape[0]):
+            first = 8 - (taps.shape[0] - 1) + tap
+            same = docs_long[first : first + rows] == docs
+            total = total + jnp.where(same, long[first : first + rows], 0.0) * taps[tap : tap + 1, span]
+        convolved = total.astype(jnp.bfloat16)
+        rate = jax.nn.sigmoid(
+            jnp.dot(convolved, rate_ref[group], preferred_element_type=jnp.float32)
+        )
+        inlet = jax.nn.sigmoid(
+            jnp.dot(convolved, inlet_ref[group], preferred_element_type=jnp.float32)
+        )
+        minus = -decay_ref[:, span]
+        soft = jnp.maximum(minus, 0.0) + jnp.log1p(jnp.exp(-jnp.abs(minus)))
+        log_decay = -RATE_SCALE * rate * soft
+        step = jnp.where(starts, 0.0, jnp.exp(log_decay))
+        factor = jnp.where(starts, 1.0, jnp.sqrt(one_minus_exp(2.0 * log_decay)))
+        state = factor * inlet * convolved.astype(jnp.float32)
+        distance = 1
+        while distance < rows:
+            state = state + step * down_by(state, distance, 0.0)
+            step = step * down_by(step, distance, 1.0)
+            distance *= 2
+        run_a[:, span] = step
+        run_b[:, span] = state
+        carry_out[:, span] = jnp.concatenate(
+            [step[rows - 1 :], state[rows - 1 :], jnp.zeros((6, LANES), jnp.float32)], axis=0
+        )
+    carry = [
+        sender(carry_out, carry_in.at[me_s], carry_s.at[k], carry_r.at[k], peer)
+        for k, peer in enumerate(sp_peers)
+    ]
+    for copy in carry:
+        copy.start()
+    carry_in[pl.ds(me_s, 1)] = carry_out[...][None]
+    raw = gate_ref[...].astype(jnp.float32)
+    gelu = 0.5 * raw * (1.0 + jnp.tanh(GELU_SCALE * (raw + 0.044715 * raw * raw * raw)))
+    gelu = gelu * gain_ref[...]
+    for copy in carry:
+        copy.wait()
+    carried = jnp.zeros((1, channels), jnp.float32)
+    for place in range(n_sp - 1):
+        tile = carry_in[place]
+        carried = jnp.where(place < me_s, tile[1:2] + tile[0:1] * carried, carried)
+    hidden = run_b[...] + run_a[...] * carried
+    row_squares = jnp.sum(hidden * hidden, axis=1, keepdims=True)
+    squares[...] = jnp.broadcast_to(row_squares, (rows, LANES)).reshape(n_tp, piece, LANES)
+    mixer = (hidden * gelu).astype(jnp.bfloat16)
+    tile_width = min(512, width)
+    for first in range(0, width, tile_width):
+        span = slice(first, first + tile_width)
+        product = jnp.dot(mixer, out_w_ref[:, span], preferred_element_type=jnp.float32)
+        parts[:, :, span] = product.astype(jnp.bfloat16).reshape(n_tp, piece, tile_width)
+
+    partner = (me_s, me_z * 2 + 1 - me_c)
+    order = [(me_z + k) % n_z for k in range(1, n_z + 1)]
+    pair = []
+    for i, z in enumerate(order):
+        theirs = z * 2 + 1 - me_c
+        pair.append(
+            (
+                sender(parts.at[theirs], pair_in.at[i], pair_s.at[0, i], pair_r.at[0, i], partner),
+                sender(
+                    squares.at[theirs], square_pair.at[i], pair_s.at[1, i], pair_r.at[1, i], partner
+                ),
+            )
+        )
+        for copy in pair[-1]:
+            copy.start()
+    z_copies = []
+    for i, z in enumerate(order):
+        mine = z * 2 + me_c
+        for copy in pair[i]:
+            copy.wait_recv()
+        z_out[i] = (
+            parts[mine].astype(jnp.float32) + pair_in[i].astype(jnp.float32)
+        ).astype(jnp.bfloat16)
+        square_out[i] = squares[mine] + square_pair[i]
+        if i < n_z - 1:
+            peer = (me_s, mine)
+            copies = (
+                sender(z_out.at[i], z_in.at[i], z_s.at[0, i], z_r.at[0, i], peer),
+                sender(square_out.at[i], square_in.at[i], z_s.at[1, i], z_r.at[1, i], peer),
+            )
+            for copy in copies:
+                copy.start()
+            z_copies.append(copies)
+    summed = z_out[n_z - 1].astype(jnp.float32)
+    square_sum = square_out[n_z - 1]
+    for i in range(n_z - 1):
+        for copy in z_copies[i]:
+            copy.wait_recv()
+        summed = summed + z_in[i].astype(jnp.float32)
+        square_sum = square_sum + square_in[i]
+    inverse = lax.rsqrt(square_sum[:, :1] / (channels * n_tp) + EPSILON)
+    residual_copy.wait()
+    own = (res_rows[...].astype(jnp.float32) + summed * inverse).astype(jnp.bfloat16)
+    own_ref[...] = own
+    floated = own.astype(jnp.float32)
+    inverse = lax.rsqrt(jnp.mean(floated * floated, axis=1, keepdims=True) + EPSILON)
+    normed_ref[...] = (floated * inverse * ffn_ref[...]).astype(jnp.bfloat16)
+    for copy in share:
+        copy.wait()
+    share_in[pl.ds(me_s, 1)] = weights_ref[...][None]
+    shares_ref[...] = share_in[...]
+    for copies in pair + z_copies:
+        for copy in copies:
+            copy.wait_send()
+
+
+def expert_kernel(
+    n_sp,
+    n_tp,
+    normed_ref,
+    own_ref,
+    shares_ref,
+    gate_hbm,
+    up_hbm,
+    down_hbm,
+    out_ref,
+    w_gate,
+    w_up,
+    w_down,
+    blocks,
+    hidden,
+    products,
+    pair_in,
+    joined,
+    first_x,
+    first_y,
+    second_x,
+    second_y,
+    relay_a,
+    relay_b,
+    column,
+    z_in,
+    w_sem,
+    own_sem,
+    gz_s,
+    gz_r,
+    gxy_s,
+    gxy_r,
+    gd_s,
+    gd_r,
+    gp_s,
+    gp_r,
+    rp_s,
+    rp_r,
+    r1_s,
+    r1_r,
+    r2_s,
+    r2_r,
+    rz_s,
+    rz_r,
+):
+    me_s, me_t = lax.axis_index("sp"), lax.axis_index("tp")
+    n_z = n_tp // 2
+    me_z, me_c = me_t // 2, me_t % 2
+    piece, width = normed_ref.shape
+    half = width // 2
+    lower, upper = pl.ds(0, half), pl.ds(half, half)
+    loads = [
+        pltpu.make_async_copy(source, target, w_sem.at[k])
+        for k, (source, target) in enumerate(
+            ((gate_hbm, w_gate), (up_hbm, w_up), (down_hbm, w_down))
+        )
+    ]
+    for copy in loads:
+        copy.start()
+    own_copy = pltpu.make_async_copy(normed_ref, blocks.at[me_s, me_t], own_sem)
+    own_copy.start()
+    s_x = me_s + 1 - 2 * (me_s % 2)
+    s_y = (me_s + 2) % n_sp
+    s_d = n_sp - 1 - me_s
+    groups = (me_s, s_x, s_y, s_d)
+    x_peer, y_peer = (s_x, me_t), (s_y, me_t)
+    partner = (me_s, me_z * 2 + 1 - me_c)
+    z_peers = [(me_s, ((me_z + k) % n_z) * 2 + me_c) for k in range(1, n_z)]
+    greet([x_peer, y_peer, partner] + z_peers)
+
+    sent = []
+
+    def push(source, target, sems, slot, peer):
+        copy = sender(source, target, sems[0].at[slot], sems[1].at[slot], peer)
+        copy.start()
+        sent.append(copy)
+        return copy
+
+    gz, gxy, gd, gp = (gz_s, gz_r), (gxy_s, gxy_r), (gd_s, gd_r), (gp_s, gp_r)
+    arrive = [((me_z + n_z - i) % n_z) * 2 + me_c for i in range(n_z)]
+    mine = blocks.at[me_s, me_t]
+    from_x, from_y, from_da, from_db, from_z = {}, {}, {}, {}, {}
+    from_pair = {}
+    for k in range(n_z - 1):
+        from_z[k + 1] = push(normed_ref, mine, gz, k, z_peers[k])
+    from_x[0] = push(normed_ref, mine, gxy, (0, 0), x_peer)
+    from_y[0] = push(normed_ref, mine, gxy, (1, 0), y_peer)
+    from_pair[0, 0] = push(normed_ref, mine, gp, (0, 0), partner)
+
+    def relay_xy(i):
+        t = arrive[i]
+        from_x[i].wait_recv()
+        block = blocks.at[s_x, t]
+        part = blocks.at[s_x, t, :, lower]
+        from_da[i] = push(part, part, gd, (0, i), y_peer)
+        from_pair[1, i] = push(block, block, gp, (1, i), partner)
+        from_y[i].wait_recv()
+        block = blocks.at[s_y, t]
+        part = blocks.at[s_y, t, :, upper]
+        from_db[i] = push(part, part, gd, (1, i), x_peer)
+        from_pair[2, i] = push(block, block, gp, (2, i), partner)
+
+    for i in range(1, n_z):
+        from_z[i].wait_recv()
+        block = blocks.at[me_s, arrive[i]]
+        from_x[i] = push(block, block, gxy, (0, i), x_peer)
+        from_y[i] = push(block, block, gxy, (1, i), y_peer)
+        from_pair[0, i] = push(block, block, gp, (0, i), partner)
+        relay_xy(i - 1)
+
+    rows = n_tp * piece
+    ff = w_gate.shape[1]
+    f_tile, d_tile = 256, min(512, width)
+    rp, r1, r2, rz = (rp_s, rp_r), (r1_s, r1_r), (r2_s, r2_r), (rz_s, rz_r)
+    send_order = [(me_z + k) % n_z for k in range(1, n_z + 1)]
+    back_pair = {}
+
+    def compute(index):
+        group = groups[index]
+        tokens = blocks[group].reshape(rows, width)
+
+        def up_step(step, _):
+            span = pl.ds(pl.multiple_of(step * f_tile, f_tile), f_tile)
+            gate_part = jnp.dot(tokens, w_gate[:, span], preferred_element_type=jnp.float32)
+            up_part = jnp.dot(tokens, w_up[:, span], preferred_element_type=jnp.float32)
+            hidden[:, span] = (gate_part * jax.nn.sigmoid(gate_part) * up_part).astype(jnp.bfloat16)
+            return 0
+
+        lax.fori_loop(0, ff // f_tile, up_step, 0)
+        share = jnp.transpose(shares_ref[group])
+        lane = lax.broadcasted_iota(jnp.int32, share.shape, 1)
+        share = jnp.sum(jnp.where(lane == me_s, share, 0.0), axis=1, keepdims=True)
+        units = hidden[...]
+
+        def down_step(step, _):
+            span = pl.ds(pl.multiple_of(step * d_tile, d_tile), d_tile)
+            product = jnp.dot(units, w_down[:, span], preferred_element_type=jnp.float32) * share
+            products[index, :, :, span] = product.astype(jnp.bfloat16).reshape(n_tp, piece, d_tile)
+            return 0
+
+        lax.fori_loop(0, width // d_tile, down_step, 0)
+        for i, z in enumerate(send_order):
+            back_pair[index, i] = push(
+                products.at[index, z * 2 + 1 - me_c], pair_in.at[index, i], rp, (index, i), partner
+            )
+
+    def join(index, i):
+        back_pair[index, i].wait_recv()
+        joined[index, i] = (
+            products[index, send_order[i] * 2 + me_c].astype(jnp.float32)
+            + pair_in[index, i].astype(jnp.float32)
+        ).astype(jnp.bfloat16)
+
+    own_copy.wait()
+    for copy in loads:
+        copy.wait()
+    for i in range(n_z):
+        from_pair[0, i].wait_recv()
+    compute(0)
+    relay_xy(n_z - 1)
+    for i in range(n_z):
+        from_pair[1, i].wait_recv()
+    compute(1)
+    for i in range(n_z):
+        t = arrive[i]
+        from_da[i].wait_recv()
+        part = blocks.at[s_d, t, :, lower]
+        from_pair[3, i] = push(part, part, gp, (3, i), partner)
+        from_db[i].wait_recv()
+        part = blocks.at[s_d, t, :, upper]
+        from_pair[4, i] = push(part, part, gp, (4, i), partner)
+    first_xs, first_ys = {}, {}
+    for i in range(n_z):
+        join(1, i)
+        first_xs[0, i] = push(
+            joined.at[1, i, :, lower], first_x.at[0, i], r1, (0, i), x_peer
+        )
+    for i in range(n_z):
+        from_pair[2, i].wait_recv()
+    compute(2)
+    for i in range(n_z):
+        join(2, i)
+        first_ys[0, i] = push(
+            joined.at[2, i, :, upper], first_y.at[0, i], r1, (1, i), y_peer
+        )
+        join(0, i)
+    for i in range(n_z):
+        from_pair[3, i].wait_recv()
+        from_pair[4, i].wait_recv()
+    compute(3)
+    for i in range(n_z):
+        join(3, i)
+        first_xs[1, i] = push(
+            joined.at[3, i, :, lower], first_x.at[1, i], r1, (2, i), x_peer
+        )
+        first_ys[1, i] = push(
+            joined.at[3, i, :, upper], first_y.at[1, i], r1, (3, i), y_peer
+        )
+    second_xs, second_ys, back_z = {}, {}, {}
+    for i in range(n_z):
+        first_xs[1, i].wait_recv()
+        relay_a[i] = (
+            joined[2, i, :, :half].astype(jnp.float32) + first_x[1, i].astype(jnp.float32)
+        ).astype(jnp.bfloat16)
+        second_ys[i] = push(relay_a.at[i], second_y.at[i], r2, (0, i), y_peer)
+        first_ys[1, i].wait_recv()
+        relay_b[i] = (
+            joined[1, i, :, half:].astype(jnp.float32) + first_y[1, i].astype(jnp.float32)
+        ).astype(jnp.bfloat16)
+        second_xs[i] = push(relay_b.at[i], second_x.at[i], r2, (1, i), x_peer)
+    for i in range(n_z):
+        first_xs[0, i].wait_recv()
+        first_ys[0, i].wait_recv()
+        second_ys[i].wait_recv()
+        second_xs[i].wait_recv()
+        low = (
+            joined[0, i, :, :half].astype(jnp.float32)
+            + first_x[0, i].astype(jnp.float32)
+            + second_y[i].astype(jnp.float32)
+        )
+        high = (
+            joined[0, i, :, half:].astype(jnp.float32)
+            + first_y[0, i].astype(jnp.float32)
+            + second_x[i].astype(jnp.float32)
+        )
+        column[i] = jnp.concatenate([low, high], axis=1).astype(jnp.bfloat16)
+        if i < n_z - 1:
+            back_z[i] = push(column.at[i], z_in.at[i], rz, i, z_peers[i])
+    total = own_ref[...].astype(jnp.float32) + column[n_z - 1].astype(jnp.float32)
+    for i in range(n_z - 1):
+        back_z[i].wait_recv()
+        total = total + z_in[i].astype(jnp.float32)
+    out_ref[...] = total.astype(jnp.bfloat16)
+    for copy in sent:
+        copy.wait_send()
+
+
+def dense_local(
+    lru_input,
+    gate_input,
+    documents,
+    conv_taps,
+    rate_weight,
+    inlet_weight,
+    decay_param,
+    lru_gain,
+    out_weight,
+    residual,
+    ffn_gain,
+    routes,
+    route_weights,
+    w_gate,
+    w_up,
+    w_down,
+):
+    n_sp, n_tp = lax.axis_size("sp"), lax.axis_size("tp")
+    n_z = n_tp // 2
+    rows, channels = lru_input.shape
+    width = residual.shape[1]
+    ff = w_gate.shape[2]
+    piece = rows // n_tp
+    padded = -(-n_sp // 8) * 8
+    docs = jnp.broadcast_to(documents[:, None], (rows, LANES))
+    expert = jnp.arange(padded, dtype=jnp.int32)[:, None]
+    shares = jnp.zeros((padded, rows), jnp.float32)
+    for k in range(routes.shape[1]):
+        shares = shares + jnp.where(
+            routes[:, k][None, :] == expert, route_weights[:, k][None, :], 0.0
+        )
+    vmem = pl.BlockSpec(memory_space=pltpu.VMEM)
+    hbm = pl.BlockSpec(memory_space=pl.ANY)
+    bf16, f32 = jnp.bfloat16, jnp.float32
+    dma = pltpu.SemaphoreType.DMA
+    own, normed, all_shares = pl.pallas_call(
+        functools.partial(front_kernel, n_sp, n_tp),
+        out_shape=(
+            jax.ShapeDtypeStruct((piece, width), bf16),
+            jax.ShapeDtypeStruct((piece, width), bf16),
+            jax.ShapeDtypeStruct((n_sp, padded, rows), f32),
+        ),
+        in_specs=[vmem] * 9 + [hbm] + [vmem] * 2,
+        out_specs=(vmem,) * 3,
+        scratch_shapes=[
+            pltpu.VMEM((16, channels), bf16),
+            pltpu.VMEM((8, LANES), jnp.int32),
+            pltpu.VMEM((8, channels), f32),
+            pltpu.VMEM((n_sp, 8, channels), f32),
+            pltpu.VMEM((n_sp, padded, rows), f32),
+            pltpu.VMEM((rows, channels), f32),
+            pltpu.VMEM((rows, channels), f32),
+            pltpu.VMEM((n_tp, piece, width), bf16),
+            pltpu.VMEM((n_z, piece, width), bf16),
+            pltpu.VMEM((n_z, piece, width), bf16),
+            pltpu.VMEM((n_z, piece, width), bf16),
+            pltpu.VMEM((n_tp, piece, LANES), f32),
+            pltpu.VMEM((n_z, piece, LANES), f32),
+            pltpu.VMEM((n_z, piece, LANES), f32),
+            pltpu.VMEM((n_z, piece, LANES), f32),
+            pltpu.VMEM((piece, width), bf16),
+            dma,
+            dma((2,)),
+            dma((2,)),
+            dma((n_sp,)),
+            dma((n_sp,)),
+            dma((n_sp,)),
+            dma((n_sp,)),
+            dma((2, n_z)),
+            dma((2, n_z)),
+            dma((2, n_z)),
+            dma((2, n_z)),
+        ],
+        compiler_params=pltpu.CompilerParams(
+            collective_id=0, has_side_effects=True, vmem_limit_bytes=40 * 2**20
+        ),
+    )(
+        lru_input,
+        gate_input,
+        docs,
+        conv_taps,
+        rate_weight,
+        inlet_weight,
+        decay_param[None, :],
+        lru_gain[None, :],
+        out_weight,
+        residual,
+        ffn_gain[None, :],
+        shares,
+    )
+    half = width // 2
+    return pl.pallas_call(
+        functools.partial(expert_kernel, n_sp, n_tp),
+        out_shape=jax.ShapeDtypeStruct((piece, width), bf16),
+        in_specs=[vmem] * 3 + [hbm] * 3,
+        out_specs=vmem,
+        scratch_shapes=[
+            pltpu.VMEM((width, ff), bf16),
+            pltpu.VMEM((width, ff), bf16),
+            pltpu.VMEM((ff, width), bf16),
+            pltpu.VMEM((n_sp, n_tp, piece, width), bf16),
+            pltpu.VMEM((rows, ff), bf16),
+            pltpu.VMEM((n_sp, n_tp, piece, width), bf16),
+            pltpu.VMEM((n_sp, n_z, piece, width), bf16),
+            pltpu.VMEM((n_sp, n_z, piece, width), bf16),
+            pltpu.VMEM((2, n_z, piece, half), bf16),
+            pltpu.VMEM((2, n_z, piece, half), bf16),
+            pltpu.VMEM((n_z, piece, half), bf16),
+            pltpu.VMEM((n_z, piece, half), bf16),
+            pltpu.VMEM((n_z, piece, half), bf16),
+            pltpu.VMEM((n_z, piece, half), bf16),
+            pltpu.VMEM((n_z, piece, width), bf16),
+            pltpu.VMEM((n_z, piece, width), bf16),
+            dma((3,)),
+            dma,
+            dma((n_z,)),
+            dma((n_z,)),
+            dma((2, n_z)),
+            dma((2, n_z)),
+            dma((2, n_z)),
+            dma((2, n_z)),
+            dma((5, n_z)),
+            dma((5, n_z)),
+            dma((4, n_z)),
+            dma((4, n_z)),
+            dma((4, n_z)),
+            dma((4, n_z)),
+            dma((2, n_z)),
+            dma((2, n_z)),
+            dma((n_z,)),
+            dma((n_z,)),
+        ],
+        compiler_params=pltpu.CompilerParams(
+            collective_id=1, has_side_effects=True, vmem_limit_bytes=60 * 2**20
+        ),
+    )(normed, own, all_shares, w_gate[0], w_up[0], w_down[0])
+
+
 def solution(mesh):
+    n_sp, n_tp = mesh.shape["sp"], mesh.shape["tp"]
+    body = dense_local if n_sp == 4 and n_tp % 2 == 0 else local
     return jax.shard_map(
-        local,
+        body,
         mesh=mesh,
         in_specs=(
             P("sp", "tp"),

time: 348 us -> 107 us (0.31); the launches traced: 344 us -> 107 us
  waiting for transfers between devices: 129 us -> 0 us
  Pallas kernels: 0 us -> 92.2 us
  local copies, waits for them, and re-layouts: 79.5 us -> 14.4 us
  other arithmetic: 44.3 us -> 0.01 us
  blocking collectives: 39.5 us -> 0 us
  matrix products: 26.1 us -> 0 us
  between operations: 13.5 us -> 0.06 us
  starting transfers between devices: 12.6 us -> 0 us
    pallas_call x0 -> x2, Pallas kernels: none -> 92.2 us  [the longest x1 66.7 us: dense_local(): pl.pallas_call(functools.partial(expert_kernel, n_sp, n_tp), out_shape=ja...]
    reduce_scatter x2 -> x0, waiting for transfers between devices: 77.2 us -> none  [the longest x1 48.8 us: local(): lax.psum_scatter(partial_out.astype(jnp.bfloat16), 'tp', scatter_dimensio...]
    slice x53 -> x2, local copies, waits for them, and re-layouts: 62.3 us -> 1.52 us  [the longest x1 0.76 us: dense_local(): routes[:, k][None, :] == expert]
    all_gather x1 -> x0, waiting for transfers between devices: 45.6 us -> none  [local(): lax.all_gather(arrived.reshape(slot_total, model_width), 'tp', axis=0, ti...]
    dot_general x6 -> x0, matrix products: 26.1 us -> none  [the longest x1 12.3 us: expert_apply(): jnp.dot(hidden_units, down_weight, preferred_element_type=jnp.float32)]
    add x28 -> x1, other arithmetic: 20.2 us -> 0.01 us  [dense_local(): shares + jnp.where(routes[:, k][None, :] == expert, route_weights[:, k][N...]
    all_gather x2 -> x0, blocking collectives: 15.1 us -> none  [carried_in(): pieces = jax.tree.map(lambda part: lax.all_gather(part, axis), value)]
    psum x1 -> x0, blocking collectives: 13.6 us -> none  [local(): square_sums = lax.psum(jnp.sum(hidden_state * hidden_state, axis=1), 'tp')]
  transfers between devices with their start and end apart: 6 -> 0, of which waited for: 4 -> 0; matrix products, arithmetic and copies ran while one was open for 2% -> 0% of each run, Pallas kernels for 0% -> 0%
where the time goes in v1:
time: 107 us
  Pallas kernels  92.2 us (86%)
  local copies, waits for them, and re-layouts  14.4 us (13%)
    pallas_call x1, Pallas kernels, dense_local(): pl.pallas_call(functools.partial(expert_kernel, n_sp, n_tp), out_shape=ja...  66.7 us
    pallas_call x1, Pallas kernels, dense_local(): pl.pallas_call(functools.partial(front_kernel, n_sp, n_tp), out_shape=(ja...  25.5 us
    unnamed x27, local copies, waits for them, and re-layouts  12.1 us

profile of v1, /device:TPU:0, one launch (start us, length us, event | category | flops | bytes accessed | tf_op | source)
XLA Modules:
  0.0 106.7 jit_solution(3603073106398977837)
XLA Ops:
  0.0 0.8 fusion
  0.8 0.8 fusion.1
  1.5 0.8 broadcast_in_dim.38.docs_ref
  2.3 0.0 copy-start
  2.3 1.2 %copy-done = bf16[256,2048]{1,0:T(8,128)(2,1)S(1)} copy-done((bf16[256,2048]{1,0:T(8,128)(2,1)S(1)}, bf16[256,2048]{1,0:T(8,128)(2,1)}, u32[]{:S(2)}) %copy-start) | copy-done | bytes 1048600
  3.5 0.0 copy-start.1
  3.5 1.2 %copy-done.1 = bf16[256,2048]{1,0:T(8,128)(2,1)S(1)} copy-done((bf16[256,2048]{1,0:T(8,128)(2,1)S(1)}, bf16[256,2048]{1,0:T(8,128)(2,1)}, u32[]{:S(2)}) %copy-start.1) | copy-done | bytes 1048600
  4.8 0.0 copy-start.4
  4.8 0.9 copy-done.4
  5.7 0.0 copy-start.5
  5.7 0.9 copy-done.5
  6.6 0.0 copy-start.6
  6.6 0.8 copy-done.6
  7.4 0.0 copy-start.7
  7.4 0.8 copy-done.7
  8.3 0.0 copy-start.9
  8.3 0.7 copy-done.9
  8.9 0.0 copy-start.10
  9.0 0.7 copy-done.10
  9.6 0.0 copy-start.11
  9.6 0.7 copy-done.11
  10.3 0.0 copy-start.12
  10.3 0.7 copy-done.12
  11.0 25.5 %shard_map.154 = (bf16[32,2048]{1,0:T(8,128)(2,1)S(1)}, bf16[32,2048]{1,0:T(8,128)(2,1)S(1)}, f32[4,8,256]{2,1,0:T(8,128)S(1)}) custom-call(bf16[256,256]{1,0:T(8,128)(2,1)S(1)} %copy-done.4, bf16[256,256]{1,0:T(8,128)(2,1)S(1)} %copy-done.5, s32[256,128]{1,0:T(8,128)S(1)} %broadcast_in_dim.38.docs_ref, bf16[4,256]{1,0:T(4,128)(2,1)S(1)} %copy-done.10, ...), custom_call_target="tpu_custom_call" | custom-call | tf_op jit(solution)/shard_map/pallas_call | solution.py:697
  36.5 0.0 copy-start.2
  36.6 0.6 copy-done.2
  37.2 0.0 copy-start.3
  37.2 0.7 copy-done.3
  37.9 0.0 copy-start.8
  37.9 0.6 copy-done.8
  38.5 66.7 %shard_map.155 = bf16[32,2048]{1,0:T(8,128)(2,1)} custom-call(bf16[32,2048]{1,0:T(8,128)(2,1)} %copy-done.3, bf16[32,2048]{1,0:T(8,128)(2,1)} %copy-done.2, f32[4,8,256]{2,1,0:T(8,128)} %copy-done.8, bf16[2048,768]{1,0:T(8,128)(2,1)} %bitcast.13, bf16[2048,768]{1,0:T(8,128)(2,1)} %bitcast.14, bf16[768,2048]{1,0:T(8,128)(2,1)} %bitcast.15), custom_call_target="tpu_custom_call" | custom-call | tf_op jit(solution)/shard_map/pallas_call | solution.py:753
  105.2 1.6 %copy.18 = bf16[32,2048]{1,0:T(8,128)(2,1)} copy(bf16[32,2048]{1,0:T(8,128)(2,1)} %shard_map.155) | data formatting | bytes 262144
  (1 shorter events, 0.0 us)
Async XLA Ops:
  2.3 1.2 %copy-start = (bf16[256,2048]{1,0:T(8,128)(2,1)S(1)}, bf16[256,2048]{1,0:T(8,128)(2,1)}, u32[]{:S(2)}) copy-start(bf16[256,2048]{1,0:T(8,128)(2,1)} %out_w_ref.1) | copy-start | bytes 3145732
  3.5 1.2 %copy-start.1 = (bf16[256,2048]{1,0:T(8,128)(2,1)S(1)}, bf16[256,2048]{1,0:T(8,128)(2,1)}, u32[]{:S(2)}) copy-start(bf16[256,2048]{1,0:T(8,128)(2,1)} %residual_ref.1) | copy-start | bytes 3145732
  4.8 0.9 copy-start.4
  5.7 0.9 copy-start.5
  6.6 0.8 copy-start.6
  7.4 0.8 copy-start.7
  8.3 0.7 copy-start.9
  8.9 0.7 copy-start.10
  9.6 0.7 copy-start.11
  10.3 0.7 copy-start.12
  36.5 0.7 copy-start.2
  37.2 0.7 copy-start.3
  37.9 0.6 copy-start.8

commit v2 on v1

--- a/solution.py
+++ b/solution.py
@@ -227,24 +227,43 @@
     return jnp.where(row >= distance, pltpu.roll(block, distance, 0), filler)
 
 
-def front_kernel(
+LATE = 8
+
+
+def layer_kernel(
     n_sp,
     n_tp,
+    lru_hbm,
+    gate_hbm,
+    docs_hbm,
+    taps_hbm,
+    rate_hbm,
+    inlet_hbm,
+    decay_hbm,
+    gain_hbm,
+    out_w_hbm,
+    residual_hbm,
+    ffn_hbm,
+    routes_hbm,
+    shares_hbm,
+    w_gate_hbm,
+    w_up_hbm,
+    w_down_hbm,
+    out_ref,
     lru_ref,
     gate_ref,
-    docs_ref,
+    docs_row,
     taps_ref,
     rate_ref,
     inlet_ref,
     decay_ref,
     gain_ref,
     out_w_ref,
-    residual_ref,
     ffn_ref,
+    routes_ref,
+    route_w_ref,
+    docs_ref,
     weights_ref,
-    own_ref,
-    normed_ref,
-    shares_ref,
     halo_x,
     halo_d,
     carry_out,
@@ -261,7 +280,29 @@
     square_out,
     square_in,
     res_rows,
+    own_ref,
+    normed_ref,
+    w_gate,
+    w_up,
+    w_down,
+    share_cols,
+    blocks,
+    hidden_units,
+    products,
+    back_in,
+    joined,
+    first_x,
+    first_y,
+    second_x,
+    second_y,
+    relay_a,
+    relay_b,
+    column,
+    last_in,
+    load_sem,
     res_sem,
+    w_sem,
+    own_sem,
     halo_s,
     halo_r,
     carry_s,
@@ -272,6 +313,22 @@
     pair_r,
     z_s,
     z_r,
+    gz_s,
+    gz_r,
+    gxy_s,
+    gxy_r,
+    gd_s,
+    gd_r,
+    gp_s,
+    gp_r,
+    rp_s,
+    rp_r,
+    r1_s,
+    r1_r,
+    r2_s,
+    r2_r,
+    rz_s,
+    rz_r,
 ):
     me_s, me_t = lax.axis_index("sp"), lax.axis_index("tp")
     n_z = n_tp // 2
@@ -279,29 +336,78 @@
     rows, channels = lru_ref.shape
     width = out_w_ref.shape[1]
     piece = rows // n_tp
+    pairs = (
+        (lru_hbm, lru_ref),
+        (docs_hbm, docs_row),
+        (taps_hbm, taps_ref),
+        (rate_hbm, rate_ref),
+        (inlet_hbm, inlet_ref),
+        (decay_hbm, decay_ref),
+        (routes_hbm, routes_ref),
+        (shares_hbm, route_w_ref),
+        (out_w_hbm, out_w_ref),
+        (gate_hbm, gate_ref),
+        (gain_hbm, gain_ref),
+        (ffn_hbm, ffn_ref),
+    )
+    loads = [
+        pltpu.make_async_copy(source, target, load_sem.at[k])
+        for k, (source, target) in enumerate(pairs)
+    ]
+    for copy in loads:
+        copy.start()
     residual_copy = pltpu.make_async_copy(
-        residual_ref.at[pl.ds(pl.multiple_of(me_t * piece, piece), piece)], res_rows, res_sem
+        residual_hbm.at[pl.ds(pl.multiple_of(me_t * piece, piece), piece)], res_rows, res_sem
     )
     residual_copy.start()
+    w_loads = [
+        pltpu.make_async_copy(source, target, w_sem.at[k])
+        for k, (source, target) in enumerate(
+            ((w_gate_hbm, w_gate), (w_up_hbm, w_up), (w_down_hbm, w_down))
+        )
+    ]
+    for copy in w_loads:
+        copy.start()
+    s_x = me_s + 1 - 2 * (me_s % 2)
+    s_y = (me_s + 2) % n_sp
+    s_d = n_sp - 1 - me_s
+    x_peer, y_peer = (s_x, me_t), (s_y, me_t)
+    partner = (me_s, me_z * 2 + 1 - me_c)
     sp_peers = [((me_s + k) % n_sp, me_t) for k in range(1, n_sp)]
-    tp_peers = [(me_s, (me_t + k) % n_tp) for k in range(1, n_tp)]
-    greet(sp_peers + tp_peers)
+    z_peers = [(me_s, ((me_z + k) % n_z) * 2 + me_c) for k in range(1, n_z)]
+    greet(sp_peers + z_peers + [partner])
+    loads[0].wait()
+    loads[1].wait()
+    docs = jnp.transpose(jnp.broadcast_to(docs_row[...], (8, rows)))
+    docs = jnp.broadcast_to(docs[:, :1], (rows, LANES))
+    docs_ref[...] = docs
     halo = [
         sender(lru_ref.at[pl.ds(rows - 16, 16)], halo_x, halo_s.at[0], halo_r.at[0], sp_peers[0]),
         sender(docs_ref.at[pl.ds(rows - 8, 8)], halo_d, halo_s.at[1], halo_r.at[1], sp_peers[0]),
     ]
     for copy in halo:
         copy.start()
+    loads[6].wait()
+    loads[7].wait()
+    expert = lax.broadcasted_iota(jnp.int32, weights_ref.shape, 0)
+    shares = jnp.zeros(weights_ref.shape, jnp.float32)
+    for k in range(routes_ref.shape[0]):
+        shares = shares + jnp.where(
+            routes_ref[k : k + 1] == expert, route_w_ref[k : k + 1], 0.0
+        )
+    weights_ref[...] = shares
     share = [
         sender(weights_ref, share_in.at[me_s], share_s.at[k], share_r.at[k], peer)
         for k, peer in enumerate(sp_peers)
     ]
     for copy in share:
         copy.start()
+    share_in[pl.ds(me_s, 1)] = shares[None]
+    for k in (2, 3, 4, 5, 9, 10, 11):
+        loads[k].wait()
     for copy in halo:
         copy.wait()
 
-    docs = docs_ref[...]
     before = jnp.where(me_s == 0, jnp.int32(-1), halo_d[...])
     docs_long = jnp.concatenate([before, docs], axis=0)
     taps = taps_ref[...].astype(jnp.float32)
@@ -358,6 +464,7 @@
     hidden = run_b[...] + run_a[...] * carried
     row_squares = jnp.sum(hidden * hidden, axis=1, keepdims=True)
     squares[...] = jnp.broadcast_to(row_squares, (rows, LANES)).reshape(n_tp, piece, LANES)
+    loads[LATE].wait()
     mixer = (hidden * gelu).astype(jnp.bfloat16)
     tile_width = min(512, width)
     for first in range(0, width, tile_width):
@@ -365,7 +472,6 @@
         product = jnp.dot(mixer, out_w_ref[:, span], preferred_element_type=jnp.float32)
         parts[:, :, span] = product.astype(jnp.bfloat16).reshape(n_tp, piece, tile_width)
 
-    partner = (me_s, me_z * 2 + 1 - me_c)
     order = [(me_z + k) % n_z for k in range(1, n_z + 1)]
     pair = []
     for i, z in enumerate(order):
@@ -412,85 +518,9 @@
     floated = own.astype(jnp.float32)
     inverse = lax.rsqrt(jnp.mean(floated * floated, axis=1, keepdims=True) + EPSILON)
     normed_ref[...] = (floated * inverse * ffn_ref[...]).astype(jnp.bfloat16)
-    for copy in share:
-        copy.wait()
-    share_in[pl.ds(me_s, 1)] = weights_ref[...][None]
-    shares_ref[...] = share_in[...]
-    for copies in pair + z_copies:
-        for copy in copies:
-            copy.wait_send()
-
-
-def expert_kernel(
-    n_sp,
-    n_tp,
-    normed_ref,
-    own_ref,
-    shares_ref,
-    gate_hbm,
-    up_hbm,
-    down_hbm,
-    out_ref,
-    w_gate,
-    w_up,
-    w_down,
-    blocks,
-    hidden,
-    products,
-    pair_in,
-    joined,
-    first_x,
-    first_y,
-    second_x,
-    second_y,
-    relay_a,
-    relay_b,
-    column,
-    z_in,
-    w_sem,
-    own_sem,
-    gz_s,
-    gz_r,
-    gxy_s,
-    gxy_r,
-    gd_s,
-    gd_r,
-    gp_s,
-    gp_r,
-    rp_s,
-    rp_r,
-    r1_s,
-    r1_r,
-    r2_s,
-    r2_r,
-    rz_s,
-    rz_r,
-):
-    me_s, me_t = lax.axis_index("sp"), lax.axis_index("tp")
-    n_z = n_tp // 2
-    me_z, me_c = me_t // 2, me_t % 2
-    piece, width = normed_ref.shape
+
     half = width // 2
     lower, upper = pl.ds(0, half), pl.ds(half, half)
-    loads = [
-        pltpu.make_async_copy(source, target, w_sem.at[k])
-        for k, (source, target) in enumerate(
-            ((gate_hbm, w_gate), (up_hbm, w_up), (down_hbm, w_down))
-        )
-    ]
-    for copy in loads:
-        copy.start()
-    own_copy = pltpu.make_async_copy(normed_ref, blocks.at[me_s, me_t], own_sem)
-    own_copy.start()
-    s_x = me_s + 1 - 2 * (me_s % 2)
-    s_y = (me_s + 2) % n_sp
-    s_d = n_sp - 1 - me_s
-    groups = (me_s, s_x, s_y, s_d)
-    x_peer, y_peer = (s_x, me_t), (s_y, me_t)
-    partner = (me_s, me_z * 2 + 1 - me_c)
-    z_peers = [(me_s, ((me_z + k) % n_z) * 2 + me_c) for k in range(1, n_z)]
-    greet([x_peer, y_peer, partner] + z_peers)
-
     sent = []
 
     def push(source, target, sems, slot, peer):
@@ -500,160 +530,172 @@
         return copy
 
     gz, gxy, gd, gp = (gz_s, gz_r), (gxy_s, gxy_r), (gd_s, gd_r), (gp_s, gp_r)
-    arrive = [((me_z + n_z - i) % n_z) * 2 + me_c for i in range(n_z)]
-    mine = blocks.at[me_s, me_t]
-    from_x, from_y, from_da, from_db, from_z = {}, {}, {}, {}, {}
-    from_pair = {}
-    for k in range(n_z - 1):
-        from_z[k + 1] = push(normed_ref, mine, gz, k, z_peers[k])
-    from_x[0] = push(normed_ref, mine, gxy, (0, 0), x_peer)
-    from_y[0] = push(normed_ref, mine, gxy, (1, 0), y_peer)
-    from_pair[0, 0] = push(normed_ref, mine, gp, (0, 0), partner)
-
-    def relay_xy(i):
-        t = arrive[i]
+    rp, r1, r2, rz = (rp_s, rp_r), (r1_s, r1_r), (r2_s, r2_r), (rz_s, rz_r)
+    from_z, from_x, from_y, from_da, from_db, from_pair = {}, {}, {}, {}, {}, {}
+
+    def spread(i):
+        block = blocks.at[i, me_s, me_c]
+        if i == 0:
+            source = normed_ref
+        else:
+            from_z[i].wait_recv()
+            source = block
+        from_x[i] = push(source, block, gxy, (0, i), x_peer)
+        from_y[i] = push(source, block, gxy, (1, i), y_peer)
+        from_pair[0, i] = push(source, block, gp, (0, i), partner)
+
+    def relay(i):
         from_x[i].wait_recv()
-        block = blocks.at[s_x, t]
-        part = blocks.at[s_x, t, :, lower]
+        block, part = blocks.at[i, s_x, me_c], blocks.at[i, s_x, me_c, :, lower]
         from_da[i] = push(part, part, gd, (0, i), y_peer)
         from_pair[1, i] = push(block, block, gp, (1, i), partner)
         from_y[i].wait_recv()
-        block = blocks.at[s_y, t]
-        part = blocks.at[s_y, t, :, upper]
+        block, part = blocks.at[i, s_y, me_c], blocks.at[i, s_y, me_c, :, upper]
         from_db[i] = push(part, part, gd, (1, i), x_peer)
         from_pair[2, i] = push(block, block, gp, (2, i), partner)
 
-    for i in range(1, n_z):
-        from_z[i].wait_recv()
-        block = blocks.at[me_s, arrive[i]]
-        from_x[i] = push(block, block, gxy, (0, i), x_peer)
-        from_y[i] = push(block, block, gxy, (1, i), y_peer)
-        from_pair[0, i] = push(block, block, gp, (0, i), partner)
-        relay_xy(i - 1)
-
-    rows = n_tp * piece
+    def hand_over(i):
+        from_da[i].wait_recv()
+        part = blocks.at[i, s_d, me_c, :, lower]
+        from_pair[3, i] = push(part, part, gp, (3, i), partner)
+        from_db[i].wait_recv()
+        part = blocks.at[i, s_d, me_c, :, upper]
+        from_pair[4, i] = push(part, part, gp, (4, i), partner)
+
+    own_copy = pltpu.make_async_copy(normed_ref, blocks.at[0, me_s, me_c], own_sem)
+    own_copy.start()
+    spread(0)
+    for k in range(n_z - 1):
+        from_z[k + 1] = push(normed_ref, blocks.at[k + 1, me_s, me_c], gz, k, z_peers[k])
+    for copy in share:
+        copy.wait()
+    for place in range(n_sp):
+        turned = jnp.transpose(share_in[place])
+        lane = lax.broadcasted_iota(jnp.int32, turned.shape, 1)
+        chosen = jnp.sum(jnp.where(lane == me_s, turned, 0.0), axis=1, keepdims=True)
+        share_cols[place] = jnp.broadcast_to(chosen, (rows, LANES))
+
     ff = w_gate.shape[1]
     f_tile, d_tile = 256, min(512, width)
-    rp, r1, r2, rz = (rp_s, rp_r), (r1_s, r1_r), (r2_s, r2_r), (rz_s, rz_r)
-    send_order = [(me_z + k) % n_z for k in range(1, n_z + 1)]
-    back_pair = {}
-
-    def compute(index):
-        group = groups[index]
-        tokens = blocks[group].reshape(rows, width)
+    count = n_sp * 2 * piece
+    back, first_xs, first_ys, second_xs, second_ys, back_z = {}, {}, {}, {}, {}, {}
+
+    def rise(i):
+        for k in range(5):
+            from_pair[k, i].wait_recv()
+        tokens = blocks[i].reshape(count, width)
 
         def up_step(step, _):
             span = pl.ds(pl.multiple_of(step * f_tile, f_tile), f_tile)
             gate_part = jnp.dot(tokens, w_gate[:, span], preferred_element_type=jnp.float32)
             up_part = jnp.dot(tokens, w_up[:, span], preferred_element_type=jnp.float32)
-            hidden[:, span] = (gate_part * jax.nn.sigmoid(gate_part) * up_part).astype(jnp.bfloat16)
+            hidden_units[:, span] = (gate_part * jax.nn.sigmoid(gate_part) * up_part).astype(
+                jnp.bfloat16
+            )
             return 0
 
         lax.fori_loop(0, ff // f_tile, up_step, 0)
-        share = jnp.transpose(shares_ref[group])
-        lane = lax.broadcasted_iota(jnp.int32, share.shape, 1)
-        share = jnp.sum(jnp.where(lane == me_s, share, 0.0), axis=1, keepdims=True)
-        units = hidden[...]
+
+    def fall(i):
+        z = (me_z + n_z - i) % n_z
+        first = pl.multiple_of(z * (2 * piece), 2 * piece)
+        scale = share_cols[:, pl.ds(first, 2 * piece), :].reshape(count, LANES)[:, :1]
+        units = hidden_units[...]
 
         def down_step(step, _):
             span = pl.ds(pl.multiple_of(step * d_tile, d_tile), d_tile)
-            product = jnp.dot(units, w_down[:, span], preferred_element_type=jnp.float32) * share
-            products[index, :, :, span] = product.astype(jnp.bfloat16).reshape(n_tp, piece, d_tile)
+            product = jnp.dot(units, w_down[:, span], preferred_element_type=jnp.float32) * scale
+            products[i, :, :, :, span] = product.astype(jnp.bfloat16).reshape(
+                n_sp, 2, piece, d_tile
+            )
             return 0
 
         lax.fori_loop(0, width // d_tile, down_step, 0)
-        for i, z in enumerate(send_order):
-            back_pair[index, i] = push(
-                products.at[index, z * 2 + 1 - me_c], pair_in.at[index, i], rp, (index, i), partner
+        for k, group in enumerate((s_d, s_x, s_y, me_s)):
+            back[k, i] = push(
+                products.at[i, group, 1 - me_c], back_in.at[i, k], rp, (k, i), partner
             )
 
-    def join(index, i):
-        back_pair[index, i].wait_recv()
-        joined[index, i] = (
-            products[index, send_order[i] * 2 + me_c].astype(jnp.float32)
-            + pair_in[index, i].astype(jnp.float32)
-        ).astype(jnp.bfloat16)
-
-    own_copy.wait()
-    for copy in loads:
-        copy.wait()
-    for i in range(n_z):
-        from_pair[0, i].wait_recv()
-    compute(0)
-    relay_xy(n_z - 1)
-    for i in range(n_z):
-        from_pair[1, i].wait_recv()
-    compute(1)
-    for i in range(n_z):
-        t = arrive[i]
-        from_da[i].wait_recv()
-        part = blocks.at[s_d, t, :, lower]
-        from_pair[3, i] = push(part, part, gp, (3, i), partner)
-        from_db[i].wait_recv()
-        part = blocks.at[s_d, t, :, upper]
-        from_pair[4, i] = push(part, part, gp, (4, i), partner)
-    first_xs, first_ys = {}, {}
-    for i in range(n_z):
-        join(1, i)
-        first_xs[0, i] = push(
-            joined.at[1, i, :, lower], first_x.at[0, i], r1, (0, i), x_peer
-        )
-    for i in range(n_z):
-        from_pair[2, i].wait_recv()
-    compute(2)
-    for i in range(n_z):
-        join(2, i)
-        first_ys[0, i] = push(
-            joined.at[2, i, :, upper], first_y.at[0, i], r1, (1, i), y_peer
-        )
-        join(0, i)
-    for i in range(n_z):
-        from_pair[3, i].wait_recv()
-        from_pair[4, i].wait_recv()
-    compute(3)
-    for i in range(n_z):
-        join(3, i)
-        first_xs[1, i] = push(
-            joined.at[3, i, :, lower], first_x.at[1, i], r1, (2, i), x_peer
-        )
-        first_ys[1, i] = push(
-            joined.at[3, i, :, upper], first_y.at[1, i], r1, (3, i), y_peer
-        )
-    second_xs, second_ys, back_z = {}, {}, {}
-    for i in range(n_z):
+    def join(i):
+        for k, group in enumerate((s_d, s_x, s_y, me_s)):
+            back[k, i].wait_recv()
+            joined[i, k] = (
+                products[i, group, me_c].astype(jnp.float32) + back_in[i, k].astype(jnp.float32)
+            ).astype(jnp.bfloat16)
+            if k == 0:
+                first_xs[1, i] = push(
+                    joined.at[i, 0, :, lower], first_x.at[1, i], r1, (2, i), x_peer
+                )
+                first_ys[1, i] = push(
+                    joined.at[i, 0, :, upper], first_y.at[1, i], r1, (3, i), y_peer
+                )
+            elif k == 1:
+                first_xs[0, i] = push(
+                    joined.at[i, 1, :, lower], first_x.at[0, i], r1, (0, i), x_peer
+                )
+            elif k == 2:
+                first_ys[0, i] = push(
+                    joined.at[i, 2, :, upper], first_y.at[0, i], r1, (1, i), y_peer
+                )
+
+    def turn(i):
         first_xs[1, i].wait_recv()
         relay_a[i] = (
-            joined[2, i, :, :half].astype(jnp.float32) + first_x[1, i].astype(jnp.float32)
+            joined[i, 2, :, :half].astype(jnp.float32) + first_x[1, i].astype(jnp.float32)
         ).astype(jnp.bfloat16)
         second_ys[i] = push(relay_a.at[i], second_y.at[i], r2, (0, i), y_peer)
         first_ys[1, i].wait_recv()
         relay_b[i] = (
-            joined[1, i, :, half:].astype(jnp.float32) + first_y[1, i].astype(jnp.float32)
+            joined[i, 1, :, half:].astype(jnp.float32) + first_y[1, i].astype(jnp.float32)
         ).astype(jnp.bfloat16)
         second_xs[i] = push(relay_b.at[i], second_x.at[i], r2, (1, i), x_peer)
-    for i in range(n_z):
-        first_xs[0, i].wait_recv()
-        first_ys[0, i].wait_recv()
-        second_ys[i].wait_recv()
-        second_xs[i].wait_recv()
+
+    def finish(i):
+        for copies in (first_xs, first_ys):
+            copies[0, i].wait_recv()
+        for copies in (second_xs, second_ys):
+            copies[i].wait_recv()
         low = (
-            joined[0, i, :, :half].astype(jnp.float32)
+            joined[i, 3, :, :half].astype(jnp.float32)
             + first_x[0, i].astype(jnp.float32)
             + second_y[i].astype(jnp.float32)
         )
         high = (
-            joined[0, i, :, half:].astype(jnp.float32)
+            joined[i, 3, :, half:].astype(jnp.float32)
             + first_y[0, i].astype(jnp.float32)
             + second_x[i].astype(jnp.float32)
         )
         column[i] = jnp.concatenate([low, high], axis=1).astype(jnp.bfloat16)
-        if i < n_z - 1:
-            back_z[i] = push(column.at[i], z_in.at[i], rz, i, z_peers[i])
-    total = own_ref[...].astype(jnp.float32) + column[n_z - 1].astype(jnp.float32)
-    for i in range(n_z - 1):
+        if i > 0:
+            peer = (me_s, ((me_z + n_z - i) % n_z) * 2 + me_c)
+            back_z[i] = push(column.at[i], last_in.at[i], rz, i, peer)
+
+    own_copy.wait()
+    for copy in w_loads:
+        copy.wait()
+    last = n_z - 1
+    for tick in range(-2, n_z + 2):
+        plan = (
+            (spread, tick + 3),
+            (relay, tick + 2),
+            (hand_over, tick + 1),
+            (rise, tick),
+            (join, tick - 1),
+            (finish, tick - 2),
+            (fall, tick),
+            (turn, tick - 1),
+        )
+        for stage, i in plan:
+            if 0 <= i <= last and not (stage is spread and i == 0):
+                stage(i)
+    total = own_ref[...].astype(jnp.float32) + column[0].astype(jnp.float32)
+    for i in range(1, n_z):
         back_z[i].wait_recv()
-        total = total + z_in[i].astype(jnp.float32)
+        total = total + last_in[i].astype(jnp.float32)
     out_ref[...] = total.astype(jnp.bfloat16)
+    for copies in pair + z_copies:
+        for copy in copies:
+            copy.wait_send()
     for copy in sent:
         copy.wait_send()
 
@@ -683,27 +725,48 @@
     ff = w_gate.shape[2]
     piece = rows // n_tp
     padded = -(-n_sp // 8) * 8
-    docs = jnp.broadcast_to(documents[:, None], (rows, LANES))
-    expert = jnp.arange(padded, dtype=jnp.int32)[:, None]
-    shares = jnp.zeros((padded, rows), jnp.float32)
-    for k in range(routes.shape[1]):
-        shares = shares + jnp.where(
-            routes[:, k][None, :] == expert, route_weights[:, k][None, :], 0.0
-        )
     vmem = pl.BlockSpec(memory_space=pltpu.VMEM)
+    half = width // 2
+    top = routes.shape[1]
     hbm = pl.BlockSpec(memory_space=pl.ANY)
     bf16, f32 = jnp.bfloat16, jnp.float32
     dma = pltpu.SemaphoreType.DMA
-    own, normed, all_shares = pl.pallas_call(
-        functools.partial(front_kernel, n_sp, n_tp),
-        out_shape=(
-            jax.ShapeDtypeStruct((piece, width), bf16),
-            jax.ShapeDtypeStruct((piece, width), bf16),
-            jax.ShapeDtypeStruct((n_sp, padded, rows), f32),
-        ),
-        in_specs=[vmem] * 9 + [hbm] + [vmem] * 2,
-        out_specs=(vmem,) * 3,
+    rows_buffer = pltpu.VMEM((n_z, piece, width), bf16)
+    half_buffer = pltpu.VMEM((n_z, piece, half), bf16)
+    chunks = pltpu.VMEM((n_z, n_sp, 2, piece, width), bf16)
+    groups = pltpu.VMEM((n_z, n_sp, piece, width), bf16)
+    square_buffer = pltpu.VMEM((n_z, piece, LANES), f32)
+    shapes = (
+        [(2,)] * 2
+        + [(n_sp,)] * 4
+        + [(2, n_z)] * 4
+        + [(n_z,)] * 2
+        + [(2, n_z)] * 4
+        + [(5, n_z)] * 2
+        + [(4, n_z)] * 4
+        + [(2, n_z)] * 2
+        + [(n_z,)] * 2
+    )
+    return pl.pallas_call(
+        functools.partial(layer_kernel, n_sp, n_tp),
+        out_shape=jax.ShapeDtypeStruct((piece, width), bf16),
+        in_specs=[hbm] * 16,
+        out_specs=vmem,
         scratch_shapes=[
+            pltpu.VMEM((rows, channels), bf16),
+            pltpu.VMEM((rows, channels), bf16),
+            pltpu.VMEM((1, rows), jnp.int32),
+            pltpu.VMEM(conv_taps.shape, bf16),
+            pltpu.VMEM(rate_weight.shape, bf16),
+            pltpu.VMEM(inlet_weight.shape, bf16),
+            pltpu.VMEM((1, channels), f32),
+            pltpu.VMEM((1, channels), f32),
+            pltpu.VMEM((channels, width), bf16),
+            pltpu.VMEM((1, width), f32),
+            pltpu.VMEM((top, rows), jnp.int32),
+            pltpu.VMEM((top, rows), f32),
+            pltpu.VMEM((rows, LANES), jnp.int32),
+            pltpu.VMEM((padded, rows), f32),
             pltpu.VMEM((16, channels), bf16),
             pltpu.VMEM((8, LANES), jnp.int32),
             pltpu.VMEM((8, channels), f32),
@@ -712,33 +775,46 @@
             pltpu.VMEM((rows, channels), f32),
             pltpu.VMEM((rows, channels), f32),
             pltpu.VMEM((n_tp, piece, width), bf16),
-            pltpu.VMEM((n_z, piece, width), bf16),
-            pltpu.VMEM((n_z, piece, width), bf16),
-            pltpu.VMEM((n_z, piece, width), bf16),
+            rows_buffer,
+            rows_buffer,
+            rows_buffer,
             pltpu.VMEM((n_tp, piece, LANES), f32),
-            pltpu.VMEM((n_z, piece, LANES), f32),
-            pltpu.VMEM((n_z, piece, LANES), f32),
-            pltpu.VMEM((n_z, piece, LANES), f32),
+            square_buffer,
+            square_buffer,
+            square_buffer,
             pltpu.VMEM((piece, width), bf16),
+            pltpu.VMEM((piece, width), bf16),
+            pltpu.VMEM((piece, width), bf16),
+            pltpu.VMEM((width, ff), bf16),
+            pltpu.VMEM((width, ff), bf16),
+            pltpu.VMEM((ff, width), bf16),
+            pltpu.VMEM((n_sp, rows, LANES), f32),
+            chunks,
+            pltpu.VMEM((n_sp * 2 * piece, ff), bf16),
+            chunks,
+            groups,
+            groups,
+            pltpu.VMEM((2, n_z, piece, half), bf16),
+            pltpu.VMEM((2, n_z, piece, half), bf16),
+            half_buffer,
+            half_buffer,
+            half_buffer,
+            half_buffer,
+            rows_buffer,
+            rows_buffer,
+            dma((12,)),
             dma,
-            dma((2,)),
-            dma((2,)),
-            dma((n_sp,)),
-            dma((n_sp,)),
-            dma((n_sp,)),
-            dma((n_sp,)),
-            dma((2, n_z)),
-            dma((2, n_z)),
-            dma((2, n_z)),
-            dma((2, n_z)),
-        ],
+            dma((3,)),
+            dma,
+        ]
+        + [dma(shape) for shape in shapes],
         compiler_params=pltpu.CompilerParams(
-            collective_id=0, has_side_effects=True, vmem_limit_bytes=40 * 2**20
+            collective_id=0, has_side_effects=True, vmem_limit_bytes=60 * 2**20
         ),
     )(
         lru_input,
         gate_input,
-        docs,
+        documents[None, :],
         conv_taps,
         rate_weight,
         inlet_weight,
@@ -747,54 +823,12 @@
         out_weight,
         residual,
         ffn_gain[None, :],
-        shares,
-    )
-    half = width // 2
-    return pl.pallas_call(
-        functools.partial(expert_kernel, n_sp, n_tp),
-        out_shape=jax.ShapeDtypeStruct((piece, width), bf16),
-        in_specs=[vmem] * 3 + [hbm] * 3,
-        out_specs=vmem,
-        scratch_shapes=[
-            pltpu.VMEM((width, ff), bf16),
-            pltpu.VMEM((width, ff), bf16),
-            pltpu.VMEM((ff, width), bf16),
-            pltpu.VMEM((n_sp, n_tp, piece, width), bf16),
-            pltpu.VMEM((rows, ff), bf16),
-            pltpu.VMEM((n_sp, n_tp, piece, width), bf16),
-            pltpu.VMEM((n_sp, n_z, piece, width), bf16),
-            pltpu.VMEM((n_sp, n_z, piece, width), bf16),
-            pltpu.VMEM((2, n_z, piece, half), bf16),
-            pltpu.VMEM((2, n_z, piece, half), bf16),
-            pltpu.VMEM((n_z, piece, half), bf16),
-            pltpu.VMEM((n_z, piece, half), bf16),
-            pltpu.VMEM((n_z, piece, half), bf16),
-            pltpu.VMEM((n_z, piece, half), bf16),
-            pltpu.VMEM((n_z, piece, width), bf16),
-            pltpu.VMEM((n_z, piece, width), bf16),
-            dma((3,)),
-            dma,
-            dma((n_z,)),
-            dma((n_z,)),
-            dma((2, n_z)),
-            dma((2, n_z)),
-            dma((2, n_z)),
-            dma((2, n_z)),
-            dma((5, n_z)),
-            dma((5, n_z)),
-            dma((4, n_z)),
-            dma((4, n_z)),
-            dma((4, n_z)),
-            dma((4, n_z)),
-            dma((2, n_z)),
-            dma((2, n_z)),
-            dma((n_z,)),
-            dma((n_z,)),
-        ],
-        compiler_params=pltpu.CompilerParams(
-            collective_id=1, has_side_effects=True, vmem_limit_bytes=60 * 2**20
-        ),
-    )(normed, own, all_shares, w_gate[0], w_up[0], w_down[0])
+        routes.T,
+        route_weights.T,
+        w_gate[0],
+        w_up[0],
+        w_down[0],
+    )
 
 
 def solution(mesh):

time: 107 us -> 90.2 us (0.84)
  local copies, waits for them, and re-layouts: 14.4 us -> 1.57 us
  Pallas kernels: 92.2 us -> 88.5 us
    unnamed x27 -> x1, local copies, waits for them, and re-layouts: 12.1 us -> 1.57 us
    pallas_call x2 -> x1, Pallas kernels: 92.2 us -> 88.5 us  [dense_local(): pl.pallas_call(functools.partial(layer_kernel, n_sp, n_tp), out_shape=jax...]
    slice x2 -> x0, local copies, waits for them, and re-layouts: 1.52 us -> none  [the longest x1 0.76 us: dense_local(): routes[:, k][None, :] == expert]
where the time goes in v2:
time: 90.2 us; the launch traced here: 90.1 us
  Pallas kernels  88.5 us (98%)
  local copies, waits for them, and re-layouts  1.57 us (2%)
    pallas_call x1, Pallas kernels, dense_local(): pl.pallas_call(functools.partial(layer_kernel, n_sp, n_tp), out_shape=jax...  88.5 us

profile of v2, /device:TPU:0, one launch (start us, length us, event | category | flops | bytes accessed | tf_op | source)
XLA Modules:
  0.0 90.1 jit_solution(127747806045708514)
XLA Ops:
  0.0 88.5 %shard_map.154 = bf16[32,2048]{1,0:T(8,128)(2,1)} custom-call(bf16[256,256]{1,0:T(8,128)(2,1)} %lru_hbm.1, bf16[256,256]{1,0:T(8,128)(2,1)} %gate_hbm.1, s32[1,256]{1,0:T(1,128)} %bitcast.15, bf16[4,256]{1,0:T(4,128)(2,1)} %taps_hbm.1, bf16[2,128,128]{2,1,0:T(8,128)(2,1)} %rate_hbm.1, bf16[2,128,128]{2,1,0:T(8,128)(2,1)} %inlet_hbm.1, f32[1,256]{1,0:T(1,128)} %bitcast.16, ...), custom_call_target="tpu_custom_call" | custom-call | tf_op jit(solution)/shard_map/pallas_call | solution.py:750
  88.5 1.6 %copy.18 = bf16[32,2048]{1,0:T(8,128)(2,1)} copy(bf16[32,2048]{1,0:T(8,128)(2,1)} %shard_map.154) | data formatting | bytes 262144

commit v3 on v2

--- a/solution.py
+++ b/solution.py
@@ -374,7 +374,8 @@
     x_peer, y_peer = (s_x, me_t), (s_y, me_t)
     partner = (me_s, me_z * 2 + 1 - me_c)
     sp_peers = [((me_s + k) % n_sp, me_t) for k in range(1, n_sp)]
-    z_peers = [(me_s, ((me_z + k) % n_z) * 2 + me_c) for k in range(1, n_z)]
+    across = (me_z, me_z + 1 - 2 * (me_z % 2), n_z - 1 - me_z, (me_z + 2) % n_z)
+    z_peers = [(me_s, across[k] * 2 + me_c) for k in range(1, n_z)]
     greet(sp_peers + z_peers + [partner])
     loads[0].wait()
     loads[1].wait()
@@ -472,7 +473,7 @@
         product = jnp.dot(mixer, out_w_ref[:, span], preferred_element_type=jnp.float32)
         parts[:, :, span] = product.astype(jnp.bfloat16).reshape(n_tp, piece, tile_width)
 
-    order = [(me_z + k) % n_z for k in range(1, n_z + 1)]
+    order = (across[2], across[3], across[1], me_z)
     pair = []
     for i, z in enumerate(order):
         theirs = z * 2 + 1 - me_c
@@ -597,7 +598,7 @@
         lax.fori_loop(0, ff // f_tile, up_step, 0)
 
     def fall(i):
-        z = (me_z + n_z - i) % n_z
+        z = across[i]
         first = pl.multiple_of(z * (2 * piece), 2 * piece)
         scale = share_cols[:, pl.ds(first, 2 * piece), :].reshape(count, LANES)[:, :1]
         units = hidden_units[...]
@@ -667,17 +668,18 @@
         )
         column[i] = jnp.concatenate([low, high], axis=1).astype(jnp.bfloat16)
         if i > 0:
-            peer = (me_s, ((me_z + n_z - i) % n_z) * 2 + me_c)
+            peer = z_peers[i - 1]
             back_z[i] = push(column.at[i], last_in.at[i], rz, i, peer)
 
     own_copy.wait()
     for copy in w_loads:
         copy.wait()
     last = n_z - 1
+    spread(1)
     for tick in range(-2, n_z + 2):
         plan = (
+            (relay, tick + 2),
             (spread, tick + 3),
-            (relay, tick + 2),
             (hand_over, tick + 1),
             (rise, tick),
             (join, tick - 1),
@@ -686,7 +688,7 @@
             (turn, tick - 1),
         )
         for stage, i in plan:
-            if 0 <= i <= last and not (stage is spread and i == 0):
+            if 0 <= i <= last and not (stage is spread and i <= 1):
                 stage(i)
     total = own_ref[...].astype(jnp.float32) + column[0].astype(jnp.float32)
     for i in range(1, n_z):
@@ -833,7 +835,7 @@
 
 def solution(mesh):
     n_sp, n_tp = mesh.shape["sp"], mesh.shape["tp"]
-    body = dense_local if n_sp == 4 and n_tp % 2 == 0 else local
+    body = dense_local if n_sp == 4 and n_tp == 8 else local
     return jax.shard_map(
         body,
         mesh=mesh,

time: 90.2 us -> 87.1 us (0.966)
  Pallas kernels: 88.5 us -> 85.4 us
    pallas_call x1, Pallas kernels: 88.5 us -> 85.4 us  [dense_local(): pl.pallas_call(functools.partial(layer_kernel, n_sp, n_tp), out_shape=jax...]
where the time goes in v3:
time: 87.1 us; the launch traced here: 86.9 us
  Pallas kernels  85.4 us (98%)
  local copies, waits for them, and re-layouts  1.57 us (2%)
    pallas_call x1, Pallas kernels, dense_local(): pl.pallas_call(functools.partial(layer_kernel, n_sp, n_tp), out_shape=jax...  85.4 us

profile of v3, /device:TPU:0, one launch (start us, length us, event | category | flops | bytes accessed | tf_op | source)
XLA Modules:
  0.0 86.9 jit_solution(9797392077727853140)
XLA Ops:
  0.0 85.4 %shard_map.154 = bf16[32,2048]{1,0:T(8,128)(2,1)} custom-call(bf16[256,256]{1,0:T(8,128)(2,1)} %lru_hbm.1, bf16[256,256]{1,0:T(8,128)(2,1)} %gate_hbm.1, s32[1,256]{1,0:T(1,128)} %bitcast.15, bf16[4,256]{1,0:T(4,128)(2,1)} %taps_hbm.1, bf16[2,128,128]{2,1,0:T(8,128)(2,1)} %rate_hbm.1, bf16[2,128,128]{2,1,0:T(8,128)(2,1)} %inlet_hbm.1, f32[1,256]{1,0:T(1,128)} %bitcast.16, ...), custom_call_target="tpu_custom_call" | custom-call | tf_op jit(solution)/shard_map/pallas_call | solution.py:752
  85.4 1.6 %copy.18 = bf16[32,2048]{1,0:T(8,128)(2,1)} copy(bf16[32,2048]{1,0:T(8,128)(2,1)} %shard_map.154) | data formatting | bytes 262144
